TPU v7x, 32 devices: a whole 2x2x4 slice. The times are simulated.
32 devices in a mesh: ep: 4 (over y, x), tp: 8 (over z, core).
Axes of the slice: x: 2, y: 2, z: 4, core: 2. Of those that a mesh axis runs over, the one named last changes fastest.
Arguments:
- tokens: bfloat16 [64, 4096], P('ep'), may hold values from -6 to 6
- attn_gain: float32 [4096], replicated, may hold values from 0.1 to 1.9
- w_query: bfloat16 [4096, 2048], P('ep', 'tp'), may hold values from -0.15625 to 0.15625
- w_key: bfloat16 [4096, 2048], P('ep', 'tp'), may hold values from -0.09375 to 0.09375
- w_value: bfloat16 [4096, 2048], P('ep', 'tp'), may hold values from -0.09375 to 0.09375
- mix_lambda: float32 [16], P('tp'), may hold values from 0.3 to 0.8
- head_gain: float32 [128], replicated, may hold values from 0.1 to 1.9
- w_output: bfloat16 [2048, 4096], P('tp'), may hold values from -0.125 to 0.125
- cache_keys: bfloat16 [64, 1024, 2048], P('ep', None, 'tp'), may hold values from -180 to 180
- cache_value: bfloat16 [64, 1024, 2048], P('ep', None, 'tp'), may hold values from -6 to 6
- lengths: int32 [64], P('ep'), may hold values from 1 to 1024
- moe_gain: float32 [4096], replicated, may hold values from 0.1 to 1.9
- group_ids: int32 [64], P('ep'), may hold values from 0 to 1, as said below
- member_ids: int32 [64, 2], P('ep'), may hold values from 0 to 1, as said below
- group_gate: float32 [64], P('ep'), may hold values from 0.3 to 1
- member_logits: float32 [64, 2], P('ep'), may hold values from -4 to 4
- w_exp_gate: bfloat16 [4, 4096, 2048], P('ep', None, 'tp'), may hold values from -0.09375 to 0.09375
- w_exp_up: bfloat16 [4, 4096, 2048], P('ep', None, 'tp'), may hold values from -0.09375 to 0.09375
- w_exp_down: bfloat16 [4, 2048, 4096], P('ep', 'tp'), may hold values from -0.125 to 0.125
Outputs:
- mixed: bfloat16 [64, 4096], P('ep', 'tp')
- fresh_keys: bfloat16 [64, 2048], P('ep', 'tp')
- fresh_value: bfloat16 [64, 2048], P('ep', 'tp')
Inputs may be any that keep to these rules, and one draw needn't show every extreme that they name: `group_ids`: each index of ep holds 16 consecutive tokens, of which every group gets the same number. A token's 2 members differ, and every expert group_ids * 2 + member_ids receives exactly 8 of the token-expert pairs of each index of ep.
All inputs are finite; a program needn't handle non-finite values.
Results may differ from a plain program's by a relative error of at most 0.015.
The roundings to bfloat16 on the way count: a program that leaves them out, or rounds other values in their place, can miss the bound.
Values may be sent and summed in bfloat16 or wider, within the bound.
A program may use at most 64 MiB of HBM per device.

v0:
```python
import functools

import jax
import jax.numpy as jnp
from jax import lax
from jax.experimental import pallas as pl
from jax.experimental.pallas import tpu as pltpu
from jax.sharding import PartitionSpec as P

EPG = 2
EPS = 1e-06
MESH = pl.DeviceIdType.MESH
F32 = jnp.float32
BF16 = jnp.bfloat16
GROUP = 4


def iota(shape, dim):
    return lax.broadcasted_iota(jnp.int32, shape, dim)


def layer_kernel(
    n_ep, n_tp, cap,
    tokens, attn_gain, head_gain, moe_gain, lam, lengths, group_ids, member_ids, group_gate, logits,
    w_query, w_key, w_value, cache_keys, cache_value, w_output, w_gate, w_up, w_down,
    mixed, fresh_keys, fresh_value,
    wq, wk, wv, kbuf, vbuf, wo, wg, wu, wd,
    nsend, nrecv, psend, precv, query, fkey, fval, head_out,
    tsend, trecv, qsend, qrecv, dsend, drecv, csend, crecv,
    w_sem, c_sem, n_ss, n_rs, p_ss, p_rs, t_ss, t_rs, q_ss, q_rs, d_ss, d_rs, e_ss, e_rs,
):
    ep = lax.axis_index("ep")
    tp = lax.axis_index("tp")
    devices = n_ep * n_tp
    me = ep * n_tp + tp
    seqs, width = tokens.shape
    rows_local = width // n_ep
    qk_cols = w_query.shape[1]
    heads_local = lam.shape[0]
    pair = qk_cols // heads_local
    head_dim = pair // 2
    total_heads = heads_local * n_tp
    positions = cache_keys.shape[1]
    cols = width // n_tp
    slot_rows = dsend.shape[1]
    slots = n_ep * slot_rows

    barrier = pltpu.get_barrier_semaphore()

    def greet(d, carry):
        other = lax.rem(me + d, devices)
        pl.semaphore_signal(
            barrier, inc=1, device_id={"ep": other // n_tp, "tp": lax.rem(other, n_tp)}, device_id_type=MESH
        )
        return carry

    lax.fori_loop(1, devices, greet, 0)

    weight_pairs = [(w_query, wq), (w_key, wk), (w_value, wv), (w_output, wo), (w_gate, wg), (w_up, wu), (w_down, wd)]

    def weight_copy(i):
        return pltpu.make_async_copy(weight_pairs[i][0], weight_pairs[i][1], w_sem.at[i])

    def cache_copy(g, kind):
        src, dst = ((cache_keys, kbuf), (cache_value, vbuf))[kind]
        rows = pl.ds(g * GROUP, GROUP)
        return pltpu.make_async_copy(src.at[rows], dst.at[rows], c_sem.at[kind, g])

    for i in range(3):
        weight_copy(i).start()
    for g in range(seqs // GROUP):
        cache_copy(g, 0).start()
        cache_copy(g, 1).start()
    for i in range(3, 7):
        weight_copy(i).start()

    resid_in = tokens[...].astype(F32)
    inv = lax.rsqrt(jnp.mean(resid_in * resid_in, axis=-1, keepdims=True) + EPS)
    normed = (resid_in * inv * attn_gain[...]).astype(BF16)
    for e in range(n_ep):
        nsend[e] = normed[:, e * rows_local : (e + 1) * rows_local]
    nrecv[ep] = nsend[ep]

    pl.semaphore_wait(barrier, devices - 1)

    def over_ep(send, recv, ss, rs, d):
        other = lax.rem(ep + d, n_ep)
        return pltpu.make_async_remote_copy(
            src_ref=send.at[other], dst_ref=recv.at[ep], send_sem=ss.at[d], recv_sem=rs.at[d],
            device_id={"ep": other, "tp": tp}, device_id_type=MESH,
        )

    for d in range(1, n_ep):
        over_ep(nsend, nrecv, n_ss, n_rs, d).start()
    for i in range(3):
        weight_copy(i).wait()
    for d in range(1, n_ep):
        over_ep(nsend, nrecv, n_ss, n_rs, d).wait_recv()
    rows_all = nrecv[...].reshape(n_ep * seqs, rows_local)
    for i, w in enumerate((wq, wk, wv)):
        part = jnp.dot(rows_all, w[...], preferred_element_type=F32)
        psend[:, :, i * qk_cols : (i + 1) * qk_cols] = part.reshape(n_ep, seqs, qk_cols)
    for d in range(1, n_ep):
        over_ep(psend, precv, p_ss, p_rs, d).start()
    precv[ep] = psend[ep]

    slot = iota((seqs, slots), 1)
    expert_of = (slot // slot_rows).astype(F32)
    rank_of = (slot % slot_rows).astype(F32)
    diagonal = iota((seqs, seqs), 0) == iota((seqs, seqs), 1)

    def column(row):
        return jnp.sum(jnp.where(diagonal, row, 0.0), axis=1, keepdims=True)

    hits = [
        column((group_ids[...] * EPG + member_ids[k : k + 1, :]).astype(F32)) == expert_of for k in range(2)
    ]
    used = (hits[0] | hits[1]).astype(BF16)
    lower = (iota((seqs, seqs), 1) < iota((seqs, seqs), 0)).astype(BF16)
    ranks = jnp.dot(lower, used, preferred_element_type=F32)
    in_slot = ranks == rank_of
    chosen = [(hits[k] & in_slot).astype(F32) for k in range(2)]
    picker = (chosen[0] + chosen[1]).T.astype(BF16)
    lg = logits[...]
    ex = jnp.exp(lg - jnp.max(lg, axis=0, keepdims=True))
    route_rows = ex / jnp.sum(ex, axis=0, keepdims=True) * group_gate[...]
    route = [column(route_rows[k : k + 1]) for k in range(2)]

    for d in range(1, n_ep):
        over_ep(psend, precv, p_ss, p_rs, d).wait_recv()
    total = precv[0]
    for e in range(1, n_ep):
        total = total + precv[e]
    projected = total.astype(BF16)
    fresh_keys[...] = projected[:, qk_cols : 2 * qk_cols]
    fresh_value[...] = projected[:, 2 * qk_cols :]
    projected = projected.astype(F32)
    query[...] = projected[:, :qk_cols]
    fkey[...] = projected[:, qk_cols : 2 * qk_cols]
    fval[...] = projected[:, 2 * qk_cols :]

    scale = head_dim ** (-0.5)
    row16 = iota((16, qk_cols), 0)
    col16 = iota((16, qk_cols), 1)
    map_mask = ((col16 // pair == row16 % 8) & ((col16 // head_dim) % 2 == row16 // 8)).astype(F32)
    head_mask = (iota((8, qk_cols), 1) // pair == iota((8, qk_cols), 0)).astype(F32)
    head_row = (tp * heads_local + iota((16, 1), 0) % 8).astype(F32)
    slopes = jnp.exp2(-8.0 * (head_row + 1.0) / total_heads)
    lam_col = jnp.zeros((8, 1), F32)
    for h in range(heads_local):
        lam_col = jnp.where(iota((8, 1), 0) == h, lam[h], lam_col)
    gain_row = jnp.concatenate([head_gain[...]] * heads_local, axis=1)
    spots = iota((1, positions), 1)

    def attend(g, carry):
        cache_copy(g, 0).wait()
        cache_copy(g, 1).wait()
        olds, news = [], []
        for i in range(GROUP):
            s = g * GROUP + i
            q16 = query[pl.ds(s, 1), :] * map_mask
            old = lax.dot_general(
                q16.astype(BF16), kbuf[s], (((1,), (1,)), ((), ())), preferred_element_type=F32
            )
            n = lengths[s]
            old = old * scale - slopes * (n - spots).astype(F32)
            olds.append(jnp.where(spots < n, old, -jnp.inf))
            news.append(jnp.sum(q16 * fkey[pl.ds(s, 1), :], axis=-1, keepdims=True) * scale)
        for i in range(GROUP):
            s = g * GROUP + i
            top = jnp.maximum(jnp.max(olds[i], axis=-1, keepdims=True), news[i])
            old = jnp.exp(olds[i] - top)
            new = jnp.exp(news[i] - top)
            recip = 1.0 / (jnp.sum(old, axis=-1, keepdims=True) + new)
            old = old * recip
            new = new * recip
            weights = (old[:8] - lam_col * old[8:]).astype(BF16)
            fresh = (new[:8] - lam_col * new[8:]).astype(BF16).astype(F32)
            mix = jnp.dot(weights, vbuf[s], preferred_element_type=F32)
            mix = (mix + fresh * fval[pl.ds(s, 1), :]) * head_mask
            mean = jnp.sum(mix * mix, axis=-1, keepdims=True) / pair
            mix = mix * lax.rsqrt(mean + EPS) * gain_row
            head_out[pl.ds(s, 1), :] = jnp.sum(mix, axis=0, keepdims=True)
        return carry

    lax.fori_loop(0, seqs // GROUP, attend, 0)

    weight_copy(3).wait()
    heads = head_out[...].astype(BF16)
    def over_tp(send, recv, ss, rs, d, same=False):
        other = lax.rem(tp + d, n_tp)
        return pltpu.make_async_remote_copy(
            src_ref=send if same else send.at[other], dst_ref=recv.at[tp], send_sem=ss.at[d], recv_sem=rs.at[d],
            device_id={"ep": ep, "tp": other}, device_id_type=MESH,
        )

    for d in [*range(1, n_tp), 0]:
        other = lax.rem(tp + d, n_tp)
        block = wo[:, pl.ds(pl.multiple_of(other * cols, cols), cols)]
        term = jnp.dot(heads, block, preferred_element_type=F32).astype(BF16)
        if d:
            tsend[other] = term
            over_tp(tsend, trecv, t_ss, t_rs, d).start()
        else:
            trecv[tp] = term
    for d in range(1, n_tp):
        over_tp(tsend, trecv, t_ss, t_rs, d).wait_recv()
    attn = trecv[0].astype(F32)
    for t in range(1, n_tp):
        attn = attn + trecv[t].astype(F32)
    my_cols = pl.ds(pl.multiple_of(tp * cols, cols), cols)
    resid = tokens[:, my_cols].astype(F32) + attn
    squares = jnp.sum(resid * resid, axis=-1, keepdims=True)
    qsend[...] = jnp.broadcast_to(squares, qsend.shape)
    for d in range(1, n_tp):
        over_tp(qsend, qrecv, q_ss, q_rs, d, True).start()
    qrecv[tp] = qsend[...]
    for d in range(1, n_tp):
        over_tp(qsend, qrecv, q_ss, q_rs, d, True).wait_recv()
    squares = qrecv[0]
    for t in range(1, n_tp):
        squares = squares + qrecv[t]
    inv = lax.rsqrt(squares[:, :1] / width + EPS)
    moe_in = (resid * inv * moe_gain[:, my_cols]).astype(BF16)
    dispatch = jnp.dot(picker, moe_in, preferred_element_type=F32)
    for e in range(n_ep):
        dsend[e] = dispatch[e * slot_rows : (e + 1) * slot_rows].astype(BF16)

    def spread(d):
        other = lax.rem(me + d, devices)
        other_ep, other_tp = other // n_tp, lax.rem(other, n_tp)
        return pltpu.make_async_remote_copy(
            src_ref=dsend.at[other_ep], dst_ref=drecv.at[tp, ep], send_sem=d_ss.at[d], recv_sem=d_rs.at[d],
            device_id={"ep": other_ep, "tp": other_tp}, device_id_type=MESH,
        )

    def gather(d):
        other_ep, other_tp = lax.rem(ep + lax.rem(d, n_ep), n_ep), lax.rem(tp + d // n_ep, n_tp)
        return pltpu.make_async_remote_copy(
            src_ref=csend.at[other_tp, other_ep], dst_ref=crecv.at[tp, ep], send_sem=e_ss.at[d], recv_sem=e_rs.at[d],
            device_id={"ep": other_ep, "tp": other_tp}, device_id_type=MESH,
        )

    def each(action):
        def step(d, carry):
            action(d)
            return carry

        lax.fori_loop(1, devices, step, 0)

    each(lambda d: spread(d).start())
    drecv[tp, ep] = dsend[ep]
    weight_copy(4).wait()
    weight_copy(5).wait()
    each(lambda d: spread(d).wait_recv())
    gate = jnp.zeros((slots, w_gate.shape[2]), F32)
    upper = gate
    for t in range(n_tp):
        rows = drecv[t].astype(F32).reshape(slots, cols).astype(BF16)
        gate = gate + jnp.dot(rows, wg[0, t * cols : (t + 1) * cols], preferred_element_type=F32)
        upper = upper + jnp.dot(rows, wu[0, t * cols : (t + 1) * cols], preferred_element_type=F32)
    hidden = (gate / (1.0 + jnp.exp(-gate)) * upper).astype(BF16)
    weight_copy(6).wait()
    for t in [*range(1, n_tp), 0]:
        other = lax.rem(tp + t, n_tp)
        block = wd[0, :, pl.ds(pl.multiple_of(other * cols, cols), cols)]
        down = jnp.dot(hidden, block, preferred_element_type=F32)
        csend[other] = down.reshape(n_ep, slot_rows, cols).astype(BF16)

        def send(e, carry, t=t):
            gather(jnp.int32(t * n_ep) + e).start()
            return carry

        lax.fori_loop(0 if t else 1, n_ep, send, 0)
    crecv[tp, ep] = csend[tp, ep]
    each(lambda d: gather(d).wait_recv())
    out = crecv[0].astype(F32)
    for t in range(1, n_tp):
        out = out + crecv[t].astype(F32)
    out = out.reshape(slots, cols).astype(BF16)
    routed = jnp.zeros((seqs, cols), F32)
    for k in range(2):
        picked = jnp.dot(chosen[k].astype(BF16), out, preferred_element_type=F32)
        routed = routed + route[k] * picked
    mixed[...] = (resid + routed).astype(BF16)

    for d in range(1, n_ep):
        over_ep(nsend, nrecv, n_ss, n_rs, d).wait_send()
        over_ep(psend, precv, p_ss, p_rs, d).wait_send()
    for d in range(1, n_tp):
        over_tp(tsend, trecv, t_ss, t_rs, d).wait_send()
        over_tp(qsend, qrecv, q_ss, q_rs, d, True).wait_send()
    each(lambda d: spread(d).wait_send())
    each(lambda d: gather(d).wait_send())


def on_device(
    tokens, attn_gain, w_query, w_key, w_value, mix_lambda, head_gain, w_output, cache_keys, cache_value,
    lengths, moe_gain, group_ids, member_ids, group_gate, member_logits, w_exp_gate, w_exp_up, w_exp_down,
):
    n_ep, n_tp = lax.axis_size("ep"), lax.axis_size("tp")
    seqs, width = tokens.shape
    qk_cols = w_query.shape[1]
    experts_all = w_exp_gate.shape[0] * n_ep
    cap = seqs * member_ids.shape[1] // experts_all
    slot_rows = -(-cap // 8) * 8
    cols = width // n_tp
    devices = n_ep * n_tp
    vmem = pl.BlockSpec(memory_space=pltpu.VMEM)
    smem = pl.BlockSpec(memory_space=pltpu.SMEM)
    hbm = pl.BlockSpec(memory_space=pl.ANY)
    dma = pltpu.SemaphoreType.DMA
    like = lambda a: pltpu.VMEM(a.shape, a.dtype)
    scratch = [
        like(w_query), like(w_key), like(w_value), like(cache_keys), like(cache_value),
        like(w_output), like(w_exp_gate), like(w_exp_up), like(w_exp_down),
        pltpu.VMEM((n_ep, seqs, width // n_ep), BF16),
        pltpu.VMEM((n_ep, seqs, width // n_ep), BF16),
        pltpu.VMEM((n_ep, seqs, 3 * qk_cols), F32),
        pltpu.VMEM((n_ep, seqs, 3 * qk_cols), F32),
        pltpu.VMEM((seqs, qk_cols), F32),
        pltpu.VMEM((seqs, qk_cols), F32),
        pltpu.VMEM((seqs, qk_cols), F32),
        pltpu.VMEM((seqs, qk_cols), F32),
        pltpu.VMEM((n_tp, seqs, cols), BF16),
        pltpu.VMEM((n_tp, seqs, cols), BF16),
        pltpu.VMEM((seqs, 128), F32),
        pltpu.VMEM((n_tp, seqs, 128), F32),
        pltpu.VMEM((n_ep, slot_rows, cols), BF16),
        pltpu.VMEM((n_tp, n_ep, slot_rows, cols), BF16),
        pltpu.VMEM((n_tp, n_ep, slot_rows, cols), BF16),
        pltpu.VMEM((n_tp, n_ep, slot_rows, cols), BF16),
        dma((7,)), dma((2, seqs // GROUP)),
        dma((n_ep,)), dma((n_ep,)), dma((n_ep,)), dma((n_ep,)),
        dma((n_tp,)), dma((n_tp,)), dma((n_tp,)), dma((n_tp,)),
        dma((devices,)), dma((devices,)), dma((devices,)), dma((devices,)),
    ]
    return pl.pallas_call(
        functools.partial(layer_kernel, n_ep, n_tp, cap),
        out_shape=(
            jax.ShapeDtypeStruct((seqs, cols), BF16),
            jax.ShapeDtypeStruct((seqs, qk_cols), BF16),
            jax.ShapeDtypeStruct((seqs, qk_cols), BF16),
        ),
        in_specs=[vmem] * 4 + [smem] * 2 + [vmem] * 4 + [hbm] * 9,
        out_specs=(vmem, vmem, vmem),
        scratch_shapes=scratch,
        compiler_params=pltpu.CompilerParams(
            collective_id=0, has_side_effects=True, vmem_limit_bytes=60 * 1024 * 1024
        ),
        name="decode_layer",
    )(
        tokens, attn_gain[None, :], head_gain[None, :], moe_gain[None, :], mix_lambda, lengths,
        group_ids[None, :], member_ids.T, group_gate[None, :], member_logits.T,
        w_query, w_key, w_value, cache_keys, cache_value, w_output, w_exp_gate, w_exp_up, w_exp_down,
    )


def solution(mesh):
    return jax.shard_map(
        on_device,
        mesh=mesh,
        in_specs=(
            P("ep", None),
            P(),
            P("ep", "tp"),
            P("ep", "tp"),
            P("ep", "tp"),
            P("tp"),
            P(),
            P("tp", None),
            P("ep", None, "tp"),
            P("ep", None, "tp"),
            P("ep"),
            P(),
            P("ep"),
            P("ep", None),
            P("ep"),
            P("ep", None),
            P("ep", None, "tp"),
            P("ep", None, "tp"),
            P("ep", "tp", None),
        ),
        out_specs=(P("ep", "tp"), P("ep", "tp"), P("ep", "tp")),
        check_vma=False,
    )
```

profile of v0, /device:TPU:0, one launch (start us, length us, event | category | flops | bytes accessed | tf_op | source)
XLA Modules:
  0.0 52.9 jit_solution(11645414794570038122)
XLA Ops:
  0.6 48.3 %decode_layer.1 = (bf16[16,512]{1,0:T(8,128)(2,1)}, bf16[16,256]{1,0:T(8,128)(2,1)}, bf16[16,256]{1,0:T(8,128)(2,1)}) custom-call(bf16[16,4096]{1,0:T(8,128)(2,1)} %tokens.1, f32[1,4096]{1,0:T(1,128)} %bitcast.7, f32[1,128]{1,0:T(1,128)} %bitcast.11, f32[1,4096]{1,0:T(1,128)} %bitcast.8, f32[2]{0:T(128)} %lam.1, s32[16]{0:T(128)} %lengths.1, ...), custom_call_target="tpu_custom_call" | custom-call | tf_op jit(solution)/shard_map/decode_layer/pallas_call | solution.py:338
  48.9 1.3 %copy.25 = bf16[16,512]{1,0:T(8,128)(2,1)} copy(bf16[16,512]{1,0:T(8,128)(2,1)} %get-tuple-element.6) | data formatting | bytes 32768
  50.3 1.3 %copy.26 = bf16[16,256]{1,0:T(8,128)(2,1)} copy(bf16[16,256]{1,0:T(8,128)(2,1)} %get-tuple-element.7) | data formatting | bytes 16384
  51.6 1.3 %copy.27 = bf16[16,256]{1,0:T(8,128)(2,1)} copy(bf16[16,256]{1,0:T(8,128)(2,1)} %get-tuple-element.8) | data formatting | bytes 16384
where the time goes:
time: 53.4 us; the launch traced here: 52.9 us
  Pallas kernels  48.3 us (90%)
  local copies, waits for them, and re-layouts  3.91 us (7%)
  between operations  0.65 us (1%)
    pallas_call x1, Pallas kernels, on_device(): pl.pallas_call(functools.partial(layer_kernel, n_ep, n_tp, cap), out_shap...  48.3 us
    unnamed x3, local copies, waits for them, and re-layouts  3.91 us

commit v1 on v0

v1 whole, which is shorter than its diff:
```python
import functools

import jax
import jax.numpy as jnp
from jax import lax
from jax.experimental import pallas as pl
from jax.experimental.pallas import tpu as pltpu
from jax.sharding import PartitionSpec as P

EPG = 2
EPS = 1e-06
MESH = pl.DeviceIdType.MESH
F32 = jnp.float32
BF16 = jnp.bfloat16
LOAD = 4
ROWS = 8


def iota(shape, dim):
    return lax.broadcasted_iota(jnp.int32, shape, dim)


def roll_rows(x, shift):
    shift = shift % ROWS
    return pltpu.roll(x, shift, 0) if shift else x


def mm(a, b):
    return jnp.dot(a, b, preferred_element_type=F32)


def layer_kernel(
    n_ep, n_tp,
    tokens_h, attn_gain_h, head_gain_h, moe_gain_h, lam_h, lengths_h, groups_h, groups_row_h, members_h, gate_h, logits_h,
    w_query, w_key, w_value, cache_keys, cache_value, w_output, w_gate, w_up, w_down,
    mixed, fresh_keys, fresh_value,
    tokens, attn_gain, head_gain, moe_gain, lam, lengths, groups, groups_row, members, group_gate, logits,
    wq, wk, wv, kbuf, vbuf, ktrans, wo, wg, wu, wd,
    nsend, nrecv, qpart, kvpart, qprecv, kvprecv, mixbuf,
    tsend, trecv, dsend, drecv, ssend, srecv, csend, crecv,
    i_sem, w_sem, c_sem, n_ss, n_rs, p_ss, p_rs, t_ss, t_rs, d_ss, d_rs, d0_rs, s_ss, s_rs, s0_rs, e_ss, e_rs, e0_rs,
):
    ep = lax.axis_index("ep")
    tp = lax.axis_index("tp")
    seqs, width = tokens.shape
    rows_local = width // n_ep
    qk_cols = w_query.shape[1]
    heads_local = lam.shape[0]
    pair = qk_cols // heads_local
    head_dim = pair // 2
    total_heads = heads_local * n_tp
    positions = cache_keys.shape[1]
    cols = width // n_tp
    waves = seqs // ROWS
    n_groups = n_ep // EPG
    hc = ROWS // n_groups
    colsp = dsend.shape[-1]
    pack = cols // colsp
    batch = ROWS // heads_local
    slots = n_ep * ROWS

    oe = [lax.rem(ep + d, n_ep) for d in range(n_ep)]
    ot = [lax.rem(tp + d, n_tp) for d in range(n_tp)]

    barrier = pltpu.get_barrier_semaphore()
    for d in range(1, n_tp):
        pl.semaphore_signal(barrier, inc=1, device_id={"ep": ep, "tp": ot[d]}, device_id_type=MESH)
    for d in range(1, n_ep):
        pl.semaphore_signal(barrier, inc=1, device_id={"ep": oe[d], "tp": tp}, device_id_type=MESH)

    small = [
        (tokens_h, tokens), (attn_gain_h, attn_gain), (head_gain_h, head_gain), (moe_gain_h, moe_gain), (lam_h, lam),
        (lengths_h, lengths), (groups_h, groups), (groups_row_h, groups_row), (members_h, members),
        (gate_h, group_gate), (logits_h, logits),
    ]
    small_copies = [pltpu.make_async_copy(s, d, i_sem.at[i]) for i, (s, d) in enumerate(small)]
    for c in small_copies:
        c.start()
    weight_pairs = [(w_query, wq), (w_key, wk), (w_value, wv), (w_output, wo), (w_gate, wg), (w_up, wu), (w_down, wd)]
    weight_copies = [pltpu.make_async_copy(s, d, w_sem.at[i]) for i, (s, d) in enumerate(weight_pairs)]

    def cache_copy(g, kind):
        src, dst = ((cache_keys, kbuf), (cache_value, vbuf))[kind]
        rows = pl.ds(g * LOAD, LOAD)
        return pltpu.make_async_copy(src.at[rows], dst.at[rows], c_sem.at[kind, g])

    for i in range(3):
        weight_copies[i].start(priority=1)
    for kind in range(2):
        for g in range(seqs // LOAD):
            cache_copy(g, kind).start(priority=1)
    for i in range(3, 7):
        weight_copies[i].start(priority=1)

    small_copies[0].wait()
    small_copies[1].wait()
    resid_in = tokens[...].astype(F32)
    inv = lax.rsqrt(jnp.mean(resid_in * resid_in, axis=-1, keepdims=True) + EPS)
    normed = (resid_in * inv * attn_gain[...]).astype(BF16)
    for e in range(n_ep):
        nsend[e] = normed[:, e * rows_local : (e + 1) * rows_local]

    def remote(src, dst, ss, rs, e, t):
        return pltpu.make_async_remote_copy(
            src_ref=src, dst_ref=dst, send_sem=ss, recv_sem=rs, device_id={"ep": e, "tp": t}, device_id_type=MESH
        )

    pl.semaphore_wait(barrier, n_ep + n_tp - 2)
    n_copies = [
        remote(nsend.at[oe[d]], nrecv.at[d], n_ss.at[d], n_rs.at[d], oe[d], tp) for d in range(1, n_ep)
    ]
    for c in n_copies:
        c.start()
    nrecv[0] = nsend[ep]

    eye = (iota((qk_cols, qk_cols), 0) == iota((qk_cols, qk_cols), 1)).astype(BF16)

    def turn(s, carry):
        flipped = lax.dot_general(eye, kbuf[s], (((1,), (1,)), ((), ())), preferred_element_type=F32)
        ktrans[s] = flipped.astype(BF16)
        return carry

    def turn_group(g, carry):
        cache_copy(g, 0).wait()
        lax.fori_loop(g * LOAD, (g + 1) * LOAD, turn, 0)
        return carry

    half = seqs // LOAD // 2
    lax.fori_loop(0, half, turn_group, 0)

    for c in weight_copies[:3]:
        c.wait()
    for c in n_copies:
        c.wait_recv()
    rows_all = nrecv[...].reshape(n_ep * seqs, rows_local)
    p_copies = []
    for i, w in enumerate((wq, wk, wv)):
        part = mm(rows_all, w[...]).reshape(n_ep, seqs, qk_cols)
        if i == 0:
            qpart[...] = part
        else:
            kvpart[:, :, (i - 1) * qk_cols : i * qk_cols] = part.astype(BF16)
    back = [lax.rem(ep + n_ep - d, n_ep) for d in range(n_ep)]
    for d in range(1, n_ep):
        p_copies.append(remote(qpart.at[d], qprecv.at[d], p_ss.at[0, d], p_rs.at[0, d], back[d], tp))
        p_copies.append(remote(kvpart.at[d], kvprecv.at[d], p_ss.at[1, d], p_rs.at[1, d], back[d], tp))
    for c in p_copies:
        c.start()

    lax.fori_loop(half, seqs // LOAD, turn_group, 0)

    for c in small_copies[2:]:
        c.wait()
    same_index = iota((seqs, seqs), 0) == iota((seqs, seqs), 1)

    def column(row):
        return jnp.sum(jnp.where(same_index, row, 0.0), axis=1, keepdims=True)

    group_row = groups_row[...].astype(F32)
    group_col = column(group_row)
    earlier = (group_col == group_row) & (iota((seqs, seqs), 0) < iota((seqs, seqs), 1))
    rank_row = jnp.sum(earlier.astype(F32), axis=0, keepdims=True)
    wave_row = jnp.floor(rank_row / hc)
    place_row = wave_row * ROWS + group_row * hc + (rank_row - wave_row * hc)
    place_col = column(place_row)
    to_place = (place_row == iota((seqs, seqs), 0).astype(F32)).astype(BF16)
    from_place = (place_col == iota((seqs, seqs), 1).astype(F32)).astype(BF16)

    ranks = []
    group_of = [groups[s] for s in range(seqs)]
    for s in range(seqs):
        r = jnp.int32(0)
        for before in range(s):
            r = r + jnp.where(group_of[before] == group_of[s], 1, 0)
        ranks.append(r)
    places = [(ranks[s] // hc) * ROWS + group_of[s] * hc + ranks[s] % hc for s in range(seqs)]
    perm = []
    for p in range(seqs):
        at = jnp.int32(0)
        for s in range(seqs):
            at = at + jnp.where(places[s] == p, s, 0)
        perm.append(at)

    lg = logits[...]
    ex = jnp.exp(lg - jnp.max(lg, axis=0, keepdims=True))
    route_rows = ex / jnp.sum(ex, axis=0, keepdims=True) * group_gate[...]
    shares = []
    for m in range(EPG):
        hit = (members[...] == m).astype(F32)
        shares.append(jnp.sum(route_rows * hit, axis=0, keepdims=True))
    row_col = iota((ROWS, 1), 0)
    slot_col = row_col % hc if pack == 2 else row_col

    def share_col(w, g, m):
        wanted = (w * ROWS + g * hc + slot_col).astype(F32)
        return jnp.sum(jnp.where(place_row == wanted, shares[m], 0.0), axis=1, keepdims=True)

    weights_of = [
        [[share_col(w, g, m) for m in range(EPG)] for g in range(n_groups)] for w in range(waves)
    ]

    my_cols = pl.ds(pl.multiple_of(tp * cols, cols), cols)
    placed_tokens = mm(to_place, tokens[:, my_cols])
    gain_part = moe_gain[:, my_cols]

    scale = head_dim ** (-0.5)
    row16 = iota((2 * ROWS, qk_cols), 0)
    col16 = iota((2 * ROWS, qk_cols), 1)
    head16 = row16 % heads_local
    map_mask = ((col16 // pair == head16) & ((col16 // head_dim) % 2 == row16 // ROWS)).astype(F32)
    seq16 = (row16 % ROWS) // heads_local
    head8 = iota((ROWS, qk_cols), 0) % heads_local
    head_mask = (iota((ROWS, qk_cols), 1) // pair == head8).astype(F32)
    seq8 = iota((ROWS, qk_cols), 0) // heads_local
    row_id = iota((2 * ROWS, 1), 0)
    slopes = jnp.exp2(-8.0 * ((tp * heads_local + row_id % heads_local).astype(F32) + 1.0) / total_heads)
    lam_col = jnp.zeros((ROWS, 1), F32)
    for h in range(heads_local):
        lam_col = jnp.where(row_col % heads_local == h, lam[h], lam_col)
    gain_row = jnp.concatenate([head_gain[...]] * heads_local, axis=1)
    spots = iota((1, positions), 1)
    pick16 = (row_id % ROWS) // heads_local

    for g in range(seqs // LOAD):
        cache_copy(g, 1).wait()

    for c in p_copies:
        c.wait_recv()
    query = qpart[0]
    fresh = kvpart[0].astype(F32)
    for d in range(1, n_ep):
        query = query + qprecv[d]
        fresh = fresh + kvprecv[d].astype(F32)
    fresh = fresh.astype(BF16)
    fresh_keys[...] = fresh[:, :qk_cols]
    fresh_value[...] = fresh[:, qk_cols:]
    projected = jnp.concatenate([query.astype(BF16), fresh], axis=1)

    weight_copies[3].wait()

    def attend(base):
        wanted = (base + pick16).astype(F32)
        spread = mm((place_row == wanted).astype(BF16), projected)
        q16 = spread[:, :qk_cols] * map_mask
        lens = jnp.zeros((2 * ROWS, 1), jnp.int32)
        old = None
        for i in range(batch):
            at = perm[base + i]
            lens = jnp.where(pick16 == i, lengths[at], lens)
            own = jnp.where(seq16 == i, q16, 0.0).astype(BF16)
            part = mm(own, ktrans[at])
            old = part if old is None else old + part
        new = jnp.sum(q16 * spread[:, qk_cols : 2 * qk_cols], axis=-1, keepdims=True) * scale
        old = old * scale - slopes * (lens - spots).astype(F32)
        old = jnp.where(spots < lens, old, -jnp.inf)
        top = jnp.maximum(jnp.max(old, axis=-1, keepdims=True), new)
        old = jnp.exp(old - top)
        new = jnp.exp(new - top)
        recip = 1.0 / (jnp.sum(old, axis=-1, keepdims=True) + new)
        old = old * recip
        new = new * recip
        weights = (old[:ROWS] - lam_col * old[ROWS:]).astype(BF16)
        fresh_weight = (new[:ROWS] - lam_col * new[ROWS:]).astype(BF16).astype(F32)
        mix = fresh_weight * spread[:ROWS, 2 * qk_cols :]
        for i in range(batch):
            part = mm(weights, vbuf[perm[base + i]])
            mix = mix + jnp.where(seq8 == i, part, 0.0)
        mix = mix * head_mask
        mean = jnp.sum(mix * mix, axis=-1, keepdims=True) / pair
        return mix * lax.rsqrt(mean + EPS) * gain_row

    t_copies = [[] for _ in range(waves)]
    for w in range(waves):
        per_wave = ROWS // batch
        for k in range(per_wave):
            mix = attend(w * ROWS + k * batch)
            for h in range(heads_local):
                mixbuf[w * heads_local + h, k * ROWS : (k + 1) * ROWS, :] = mix[:, h * pair : (h + 1) * pair]
        heads = [
            mixbuf[w * heads_local + h, pl.ds(h, ROWS, stride=heads_local), :] for h in range(heads_local)
        ]
        heads = jnp.concatenate(heads, axis=1).astype(BF16)
        for d in [*range(1, n_tp), 0]:
            block = wo[:, pl.ds(pl.multiple_of(ot[d] * cols, cols), cols)]
            term = mm(heads, block).astype(BF16)
            if d:
                tsend[w, d] = term
                c = remote(tsend.at[w, d], trecv.at[w, d], t_ss.at[w, d], t_rs.at[w, d], ep, ot[d])
                c.start()
                t_copies[w].append(c)
            else:
                trecv[w, 0] = term

    rows_of = iota((ROWS, colsp), 0)
    resid = []
    d_copies = [[] for _ in range(waves)]
    for w in range(waves):
        for c in t_copies[w]:
            c.wait_recv()
        attn = trecv[w, 0].astype(F32)
        for d in range(1, n_tp):
            attn = attn + trecv[w, d].astype(F32)
        res = placed_tokens[w * ROWS : (w + 1) * ROWS] + attn
        resid.append(res)
        rows = res * gain_part
        for g in range(n_groups):
            if pack == 2:
                first = roll_rows(rows[:, :colsp], -g * hc)
                second = roll_rows(rows[:, colsp:], hc - g * hc)
                dsend[w, g] = jnp.where(rows_of < hc, first, second).astype(BF16)
            else:
                dsend[w, g] = roll_rows(rows, -g * hc).astype(BF16)
        squares = jnp.sum(res * res, axis=-1, keepdims=True)
        wide = jnp.where(iota((ROWS, 128), 0) == iota((ROWS, 128), 1), squares, 0.0)
        ssend[w] = jnp.sum(wide, axis=0, keepdims=True)
        for t in [*range(1, n_tp), 0]:
            for e in range(n_ep):
                if t or e:
                    d_rs_at = d_rs.at[w, t] if t else d0_rs.at[w, e]
                    s_rs_at = s_rs.at[w, t] if t else s0_rs.at[w, e]
                    c = remote(dsend.at[w, oe[e] // EPG], drecv.at[w, t, e], d_ss.at[w, t, e], d_rs_at, oe[e], ot[t])
                    c.start()
                    s = remote(ssend.at[w], srecv.at[w, t, e], s_ss.at[w, t, e], s_rs_at, oe[e], ot[t])
                    s.start()
                    d_copies[w] += [c, s]
        drecv[w, 0, 0] = dsend[w, ep // EPG]
        srecv[w, 0, 0] = ssend[w]

    def slab_wait(ref, sem):
        pltpu.make_async_copy(ref, ref, sem).wait()

    e_copies = [[] for _ in range(waves)]
    rows32 = iota((slots, w_gate.shape[2]), 0) % ROWS
    for i in range(4, 7):
        weight_copies[i].wait()
    for w in range(waves):
        hid = w_gate.shape[2]
        gates = [jnp.zeros((slots, hid), F32) for _ in range(pack)]
        uppers = [jnp.zeros((slots, hid), F32) for _ in range(pack)]
        for t in range(n_tp):
            if t:
                slab_wait(drecv.at[w, t], d_rs.at[w, t])
            else:
                for e in range(1, n_ep):
                    slab_wait(drecv.at[w, 0, e], d0_rs.at[w, e])
            x = drecv[w, t].reshape(slots, colsp)
            source = lax.rem(tp + n_tp - t, n_tp)
            for p in range(pack):
                at = pl.ds(pl.multiple_of(source * cols + p * colsp, colsp), colsp)
                gates[p] = gates[p] + mm(x, wg[0, at])
                uppers[p] = uppers[p] + mm(x, wu[0, at])
        for t in range(n_tp):
            if t:
                slab_wait(srecv.at[w, t], s_rs.at[w, t])
            else:
                for e in range(1, n_ep):
                    slab_wait(srecv.at[w, 0, e], s0_rs.at[w, e])
        squares = srecv[w, 0]
        for t in range(1, n_tp):
            squares = squares + srecv[w, t]
        squares = jnp.broadcast_to(squares, (n_ep, ROWS, 128)).reshape(slots, 128)
        slot = iota((slots, 128), 0) % ROWS
        if pack == 2:
            slot = slot % hc
        lane = (ep // EPG) * hc + slot
        lane = lax.rem(lane, ROWS)
        squares = jnp.sum(jnp.where(iota((slots, 128), 1) == lane, squares, 0.0), axis=-1, keepdims=True)
        inv = lax.rsqrt(squares / width + EPS)

        def join(parts):
            if pack == 1:
                return parts[0]
            down_shift = pltpu.roll(parts[1], slots - hc, 0)
            up_shift = pltpu.roll(parts[0], hc, 0)
            return jnp.where(rows32 < hc, parts[0] + down_shift, parts[1] + up_shift)

        gate = join(gates) * inv
        upper = join(uppers) * inv
        hidden = (gate / (1.0 + jnp.exp(-gate)) * upper).astype(BF16)
        for t in [*range(1, n_tp), 0]:
            downs = [
                mm(hidden, wd[0, :, pl.ds(pl.multiple_of(ot[t] * cols + p * colsp, colsp), colsp)]) for p in range(pack)
            ]
            down = downs[0] if pack == 1 else jnp.where(iota((slots, colsp), 0) % ROWS < hc, downs[0], downs[1])
            down = down.reshape(n_ep, ROWS, colsp).astype(BF16)
            csend[w, t] = down
            for e in range(n_ep):
                if t or e:
                    e_rs_at = e_rs.at[w, t] if t else e0_rs.at[w, e]
                    c = remote(csend.at[w, t, e], crecv.at[w, t, ep], e_ss.at[w, t, e], e_rs_at, back[e], ot[t])
                    c.start()
                    e_copies[w].append(c)
        crecv[w, 0, ep] = csend[w, 0, 0]

    for c in n_copies + p_copies:
        c.wait_send()
    for w in range(waves):
        for c in t_copies[w] + d_copies[w] + e_copies[w]:
            c.wait_send()

    final = None
    for w in range(waves):
        for t in range(n_tp):
            if t:
                slab_wait(crecv.at[w, t], e_rs.at[w, t])
            else:
                for e in range(1, n_ep):
                    slab_wait(crecv.at[w, 0, e], e0_rs.at[w, e])
        routed = [jnp.zeros((ROWS, colsp), F32) for _ in range(pack)]
        for g in range(n_groups):
            total = jnp.zeros((ROWS, colsp), F32)
            for m in range(EPG):
                e = g * EPG + m
                out = crecv[w, 0, e].astype(F32)
                for t in range(1, n_tp):
                    out = out + crecv[w, t, e].astype(F32)
                total = total + weights_of[w][g][m] * out.astype(BF16).astype(F32)
            for p in range(pack):
                routed[p] = jnp.where(rows_of // hc == g, roll_rows(total, g * hc - p * hc), routed[p])
        routed = routed[0] if pack == 1 else jnp.concatenate(routed, axis=1)
        placed = (resid[w] + routed).astype(BF16)
        part = mm(from_place[:, w * ROWS : (w + 1) * ROWS], placed)
        final = part if final is None else final + part
    mixed[...] = final.astype(BF16)


def finish_kernel(a, b, c, x, y, z):
    x[...] = a[...]
    y[...] = b[...]
    z[...] = c[...]


def on_device(
    tokens, attn_gain, w_query, w_key, w_value, mix_lambda, head_gain, w_output, cache_keys, cache_value,
    lengths, moe_gain, group_ids, member_ids, group_gate, member_logits, w_exp_gate, w_exp_up, w_exp_down,
):
    n_ep, n_tp = lax.axis_size("ep"), lax.axis_size("tp")
    seqs, width = tokens.shape
    qk_cols = w_query.shape[1]
    heads_local = mix_lambda.shape[0]
    cols = width // n_tp
    waves = seqs // ROWS
    n_groups = n_ep // EPG
    hc = ROWS // n_groups
    pack = 2 if hc * 2 == ROWS and cols % 256 == 0 else 1
    colsp = cols // pack
    vmem = pl.BlockSpec(memory_space=pltpu.VMEM)
    hbm = pl.BlockSpec(memory_space=pl.ANY)
    dma = pltpu.SemaphoreType.DMA
    like = lambda a: pltpu.VMEM(a.shape, a.dtype)
    operands = (
        tokens, attn_gain[None, :], head_gain[None, :], moe_gain[None, :], mix_lambda, lengths, group_ids,
        group_ids[None, :], member_ids.T, group_gate[None, :], member_logits.T,
        w_query, w_key, w_value, cache_keys, cache_value, w_output, w_exp_gate, w_exp_up, w_exp_down,
    )
    held = [
        pltpu.SMEM(a.shape, a.dtype) if i in (4, 5, 6) else like(a) for i, a in enumerate(operands[:11])
    ]
    scratch = held + [
        like(w_query), like(w_key), like(w_value), like(cache_keys), like(cache_value),
        pltpu.VMEM((seqs, qk_cols, cache_keys.shape[1]), BF16),
        like(w_output), like(w_exp_gate), like(w_exp_up), like(w_exp_down),
        pltpu.VMEM((n_ep, seqs, width // n_ep), BF16),
        pltpu.VMEM((n_ep, seqs, width // n_ep), BF16),
        pltpu.VMEM((n_ep, seqs, qk_cols), F32),
        pltpu.VMEM((n_ep, seqs, 2 * qk_cols), BF16),
        pltpu.VMEM((n_ep, seqs, qk_cols), F32),
        pltpu.VMEM((n_ep, seqs, 2 * qk_cols), BF16),
        pltpu.VMEM((waves * heads_local, ROWS * heads_local, qk_cols // heads_local), F32),
        pltpu.VMEM((waves, n_tp, ROWS, cols), BF16),
        pltpu.VMEM((waves, n_tp, ROWS, cols), BF16),
        pltpu.VMEM((waves, n_groups, ROWS, colsp), BF16),
        pltpu.VMEM((waves, n_tp, n_ep, ROWS, colsp), BF16),
        pltpu.VMEM((waves, 1, 128), F32),
        pltpu.VMEM((waves, n_tp, n_ep, 1, 128), F32),
        pltpu.VMEM((waves, n_tp, n_ep, ROWS, colsp), BF16),
        pltpu.VMEM((waves, n_tp, n_ep, ROWS, colsp), BF16),
        dma((11,)), dma((7,)), dma((2, seqs // LOAD)),
        dma((n_ep,)), dma((n_ep,)), dma((2, n_ep)), dma((2, n_ep)),
        dma((waves, n_tp)), dma((waves, n_tp)),
        dma((waves, n_tp, n_ep)), dma((waves, n_tp)), dma((waves, n_ep)),
        dma((waves, n_tp, n_ep)), dma((waves, n_tp)), dma((waves, n_ep)),
        dma((waves, n_tp, n_ep)), dma((waves, n_tp)), dma((waves, n_ep)),
    ]
    shapes = (
        jax.ShapeDtypeStruct((seqs, cols), BF16),
        jax.ShapeDtypeStruct((seqs, qk_cols), BF16),
        jax.ShapeDtypeStruct((seqs, qk_cols), BF16),
    )
    results = pl.pallas_call(
        functools.partial(layer_kernel, n_ep, n_tp),
        out_shape=shapes,
        in_specs=[hbm] * len(operands),
        out_specs=(vmem, vmem, vmem),
        scratch_shapes=scratch,
        compiler_params=pltpu.CompilerParams(
            collective_id=0, has_side_effects=True, vmem_limit_bytes=60 * 1024 * 1024
        ),
        name="decode_layer",
    )(*operands)
    return pl.pallas_call(
        finish_kernel, out_shape=shapes, in_specs=[vmem] * 3, out_specs=(vmem,) * 3, name="finish"
    )(*results)


def solution(mesh):
    return jax.shard_map(
        on_device,
        mesh=mesh,
        in_specs=(
            P("ep", None),
            P(),
            P("ep", "tp"),
            P("ep", "tp"),
            P("ep", "tp"),
            P("tp"),
            P(),
            P("tp", None),
            P("ep", None, "tp"),
            P("ep", None, "tp"),
            P("ep"),
            P(),
            P("ep"),
            P("ep", None),
            P("ep"),
            P("ep", None),
            P("ep", None, "tp"),
            P("ep", None, "tp"),
            P("ep", "tp", None),
        ),
        out_specs=(P("ep", "tp"), P("ep", "tp"), P("ep", "tp")),
        check_vma=False,
    )
```

time: 53.4 us -> 40.9 us (0.77)
  Pallas kernels: 48.3 us -> 40 us
  local copies, waits for them, and re-layouts: 3.91 us -> 0 us
    pallas_call x1 -> x2, Pallas kernels: 48.3 us -> 40 us  [the longest x1 38.7 us: on_device(): pl.pallas_call(functools.partial(layer_kernel, n_ep, n_tp), out_shape=sha...]
    unnamed x3 -> x0, local copies, waits for them, and re-layouts: 3.91 us -> none
where the time goes in v1:
time: 40.9 us; the launch traced here: 40.7 us
  Pallas kernels  40 us (98%)
  between operations  0.65 us (2%)
    pallas_call x1, Pallas kernels, on_device(): pl.pallas_call(functools.partial(layer_kernel, n_ep, n_tp), out_shape=sha...  38.7 us
    pallas_call x1, Pallas kernels, on_device(): pl.pallas_call(finish_kernel, out_shape=shapes, in_specs=[vmem] * 3, out_...  1.35 us

profile of v1, /device:TPU:0, one launch (start us, length us, event | category | flops | bytes accessed | tf_op | source)
XLA Modules:
  0.0 40.7 jit_solution(1829511380728186228)
XLA Ops:
  0.6 38.7 %decode_layer.1 = (bf16[16,512]{1,0:T(8,128)(2,1)}, bf16[16,256]{1,0:T(8,128)(2,1)}, bf16[16,256]{1,0:T(8,128)(2,1)}) custom-call(bf16[16,4096]{1,0:T(8,128)(2,1)} %tokens_h.1, f32[1,4096]{1,0:T(1,128)} %bitcast.7, f32[1,128]{1,0:T(1,128)} %bitcast.12, f32[1,4096]{1,0:T(1,128)} %bitcast.8, f32[2]{0:T(128)} %lam_h.1, s32[16]{0:T(128)} %lengths_h.1, ...), custom_call_target="tpu_custom_call" | custom-call | tf_op jit(solution)/shard_map/decode_layer/pallas_call | solution.py:490
  39.3 1.4 %finish.1 = (bf16[16,512]{1,0:T(8,128)(2,1)}, bf16[16,256]{1,0:T(8,128)(2,1)}, bf16[16,256]{1,0:T(8,128)(2,1)}) custom-call(bf16[16,512]{1,0:T(8,128)(2,1)} %get-tuple-element.6.a, bf16[16,256]{1,0:T(8,128)(2,1)} %get-tuple-element.7.b, bf16[16,256]{1,0:T(8,128)(2,1)} %get-tuple-element.8.c), custom_call_target="tpu_custom_call" | custom-call | tf_op jit(solution)/shard_map/finish/pallas_call | solution.py:501

commit v2 on v1

--- a/solution.py
+++ b/solution.py
@@ -38,7 +38,7 @@
     wq, wk, wv, kbuf, vbuf, ktrans, wo, wg, wu, wd,
     nsend, nrecv, qpart, kvpart, qprecv, kvprecv, mixbuf,
     tsend, trecv, dsend, drecv, ssend, srecv, csend, crecv,
-    i_sem, w_sem, c_sem, n_ss, n_rs, p_ss, p_rs, t_ss, t_rs, d_ss, d_rs, d0_rs, s_ss, s_rs, s0_rs, e_ss, e_rs, e0_rs,
+    i_sem, w_sem, c_sem, n_sem, p_sem, t_sem, d_ss, d_rs, s_sem, e_sem,
 ):
     ep = lax.axis_index("ep")
     tp = lax.axis_index("tp")
@@ -79,16 +79,17 @@
     weight_pairs = [(w_query, wq), (w_key, wk), (w_value, wv), (w_output, wo), (w_gate, wg), (w_up, wu), (w_down, wd)]
     weight_copies = [pltpu.make_async_copy(s, d, w_sem.at[i]) for i, (s, d) in enumerate(weight_pairs)]
 
-    def cache_copy(g, kind):
-        src, dst = ((cache_keys, kbuf), (cache_value, vbuf))[kind]
+    def key_copy(g):
         rows = pl.ds(g * LOAD, LOAD)
-        return pltpu.make_async_copy(src.at[rows], dst.at[rows], c_sem.at[kind, g])
+        return pltpu.make_async_copy(cache_keys.at[rows], kbuf.at[rows], c_sem.at[g])
+
+    value_copy = pltpu.make_async_copy(cache_value, vbuf, c_sem.at[seqs // LOAD])
 
     for i in range(3):
         weight_copies[i].start(priority=1)
-    for kind in range(2):
-        for g in range(seqs // LOAD):
-            cache_copy(g, kind).start(priority=1)
+    for g in range(seqs // LOAD):
+        key_copy(g).start(priority=1)
+    value_copy.start(priority=1)
     for i in range(3, 7):
         weight_copies[i].start(priority=1)
 
@@ -106,11 +107,11 @@
         )
 
     pl.semaphore_wait(barrier, n_ep + n_tp - 2)
-    n_copies = [
-        remote(nsend.at[oe[d]], nrecv.at[d], n_ss.at[d], n_rs.at[d], oe[d], tp) for d in range(1, n_ep)
-    ]
-    for c in n_copies:
-        c.start()
+    def slab_wait(ref, sem):
+        pltpu.make_async_copy(ref, ref, sem).wait()
+
+    for d in range(1, n_ep):
+        remote(nsend.at[oe[d]], nrecv.at[d], n_sem.at[0], n_sem.at[1], oe[d], tp).start()
     nrecv[0] = nsend[ep]
 
     eye = (iota((qk_cols, qk_cols), 0) == iota((qk_cols, qk_cols), 1)).astype(BF16)
@@ -121,7 +122,7 @@
         return carry
 
     def turn_group(g, carry):
-        cache_copy(g, 0).wait()
+        key_copy(g).wait()
         lax.fori_loop(g * LOAD, (g + 1) * LOAD, turn, 0)
         return carry
 
@@ -130,10 +131,8 @@
 
     for c in weight_copies[:3]:
         c.wait()
-    for c in n_copies:
-        c.wait_recv()
+    slab_wait(nrecv.at[1:n_ep], n_sem.at[1])
     rows_all = nrecv[...].reshape(n_ep * seqs, rows_local)
-    p_copies = []
     for i, w in enumerate((wq, wk, wv)):
         part = mm(rows_all, w[...]).reshape(n_ep, seqs, qk_cols)
         if i == 0:
@@ -142,10 +141,8 @@
             kvpart[:, :, (i - 1) * qk_cols : i * qk_cols] = part.astype(BF16)
     back = [lax.rem(ep + n_ep - d, n_ep) for d in range(n_ep)]
     for d in range(1, n_ep):
-        p_copies.append(remote(qpart.at[d], qprecv.at[d], p_ss.at[0, d], p_rs.at[0, d], back[d], tp))
-        p_copies.append(remote(kvpart.at[d], kvprecv.at[d], p_ss.at[1, d], p_rs.at[1, d], back[d], tp))
-    for c in p_copies:
-        c.start()
+        remote(qpart.at[d], qprecv.at[d], p_sem.at[0], p_sem.at[1], back[d], tp).start()
+        remote(kvpart.at[d], kvprecv.at[d], p_sem.at[2], p_sem.at[3], back[d], tp).start()
 
     lax.fori_loop(half, seqs // LOAD, turn_group, 0)
 
@@ -221,11 +218,10 @@
     spots = iota((1, positions), 1)
     pick16 = (row_id % ROWS) // heads_local
 
-    for g in range(seqs // LOAD):
-        cache_copy(g, 1).wait()
-
-    for c in p_copies:
-        c.wait_recv()
+    value_copy.wait()
+
+    slab_wait(qprecv.at[1:n_ep], p_sem.at[1])
+    slab_wait(kvprecv.at[1:n_ep], p_sem.at[3])
     query = qpart[0]
     fresh = kvpart[0].astype(F32)
     for d in range(1, n_ep):
@@ -269,7 +265,6 @@
         mean = jnp.sum(mix * mix, axis=-1, keepdims=True) / pair
         return mix * lax.rsqrt(mean + EPS) * gain_row
 
-    t_copies = [[] for _ in range(waves)]
     for w in range(waves):
         per_wave = ROWS // batch
         for k in range(per_wave):
@@ -285,18 +280,16 @@
             term = mm(heads, block).astype(BF16)
             if d:
                 tsend[w, d] = term
-                c = remote(tsend.at[w, d], trecv.at[w, d], t_ss.at[w, d], t_rs.at[w, d], ep, ot[d])
-                c.start()
-                t_copies[w].append(c)
+                remote(tsend.at[w, d], trecv.at[w, d], t_sem.at[0, w], t_sem.at[1, w], ep, ot[d]).start()
             else:
                 trecv[w, 0] = term
 
     rows_of = iota((ROWS, colsp), 0)
     resid = []
-    d_copies = [[] for _ in range(waves)]
+    parts = d_rs.shape[1]
+    others = n_tp * n_ep
     for w in range(waves):
-        for c in t_copies[w]:
-            c.wait_recv()
+        slab_wait(trecv.at[w, 1:n_tp], t_sem.at[1, w])
         attn = trecv[w, 0].astype(F32)
         for d in range(1, n_tp):
             attn = attn + trecv[w, d].astype(F32)
@@ -316,20 +309,13 @@
         for t in [*range(1, n_tp), 0]:
             for e in range(n_ep):
                 if t or e:
-                    d_rs_at = d_rs.at[w, t] if t else d0_rs.at[w, e]
-                    s_rs_at = s_rs.at[w, t] if t else s0_rs.at[w, e]
-                    c = remote(dsend.at[w, oe[e] // EPG], drecv.at[w, t, e], d_ss.at[w, t, e], d_rs_at, oe[e], ot[t])
-                    c.start()
-                    s = remote(ssend.at[w], srecv.at[w, t, e], s_ss.at[w, t, e], s_rs_at, oe[e], ot[t])
-                    s.start()
-                    d_copies[w] += [c, s]
-        drecv[w, 0, 0] = dsend[w, ep // EPG]
-        srecv[w, 0, 0] = ssend[w]
-
-    def slab_wait(ref, sem):
-        pltpu.make_async_copy(ref, ref, sem).wait()
-
-    e_copies = [[] for _ in range(waves)]
+                    at = t * n_ep + e
+                    arrived = d_rs.at[w, t * parts // n_tp]
+                    remote(dsend.at[w, oe[e] // EPG], drecv.at[w, at], d_ss.at[w], arrived, oe[e], ot[t]).start()
+                    remote(ssend.at[w], srecv.at[w, at], s_sem.at[0, w], s_sem.at[1, w], oe[e], ot[t]).start()
+        drecv[w, 0] = dsend[w, ep // EPG]
+        srecv[w, 0] = ssend[w]
+
     rows32 = iota((slots, w_gate.shape[2]), 0) % ROWS
     for i in range(4, 7):
         weight_copies[i].wait()
@@ -338,26 +324,19 @@
         gates = [jnp.zeros((slots, hid), F32) for _ in range(pack)]
         uppers = [jnp.zeros((slots, hid), F32) for _ in range(pack)]
         for t in range(n_tp):
-            if t:
-                slab_wait(drecv.at[w, t], d_rs.at[w, t])
-            else:
-                for e in range(1, n_ep):
-                    slab_wait(drecv.at[w, 0, e], d0_rs.at[w, e])
-            x = drecv[w, t].reshape(slots, colsp)
+            step = n_tp // parts
+            if t % step == 0:
+                slab_wait(drecv.at[w, max(t * n_ep, 1) : (t + step) * n_ep], d_rs.at[w, t // step])
+            x = drecv[w, t * n_ep : (t + 1) * n_ep].reshape(slots, colsp)
             source = lax.rem(tp + n_tp - t, n_tp)
             for p in range(pack):
                 at = pl.ds(pl.multiple_of(source * cols + p * colsp, colsp), colsp)
                 gates[p] = gates[p] + mm(x, wg[0, at])
                 uppers[p] = uppers[p] + mm(x, wu[0, at])
-        for t in range(n_tp):
-            if t:
-                slab_wait(srecv.at[w, t], s_rs.at[w, t])
-            else:
-                for e in range(1, n_ep):
-                    slab_wait(srecv.at[w, 0, e], s0_rs.at[w, e])
-        squares = srecv[w, 0]
+        slab_wait(srecv.at[w, 1:others], s_sem.at[1, w])
+        squares = srecv[w, 0:n_ep]
         for t in range(1, n_tp):
-            squares = squares + srecv[w, t]
+            squares = squares + srecv[w, t * n_ep : (t + 1) * n_ep]
         squares = jnp.broadcast_to(squares, (n_ep, ROWS, 128)).reshape(slots, 128)
         slot = iota((slots, 128), 0) % ROWS
         if pack == 2:
@@ -383,37 +362,33 @@
             ]
             down = downs[0] if pack == 1 else jnp.where(iota((slots, colsp), 0) % ROWS < hc, downs[0], downs[1])
             down = down.reshape(n_ep, ROWS, colsp).astype(BF16)
-            csend[w, t] = down
+            csend[w, t * n_ep : (t + 1) * n_ep] = down
             for e in range(n_ep):
                 if t or e:
-                    e_rs_at = e_rs.at[w, t] if t else e0_rs.at[w, e]
-                    c = remote(csend.at[w, t, e], crecv.at[w, t, ep], e_ss.at[w, t, e], e_rs_at, back[e], ot[t])
-                    c.start()
-                    e_copies[w].append(c)
-        crecv[w, 0, ep] = csend[w, 0, 0]
-
-    for c in n_copies + p_copies:
-        c.wait_send()
+                    at = t * n_ep + e
+                    remote(csend.at[w, at], crecv.at[w, at], e_sem.at[0, w], e_sem.at[1, w], back[e], ot[t]).start()
+        crecv[w, 0] = csend[w, 0]
+
+    slab_wait(nsend.at[1:n_ep], n_sem.at[0])
+    slab_wait(qpart.at[1:n_ep], p_sem.at[0])
+    slab_wait(kvpart.at[1:n_ep], p_sem.at[2])
     for w in range(waves):
-        for c in t_copies[w] + d_copies[w] + e_copies[w]:
-            c.wait_send()
+        slab_wait(tsend.at[w, 1:n_tp], t_sem.at[0, w])
+        slab_wait(drecv.at[w, 1:others], d_ss.at[w])
+        slab_wait(srecv.at[w, 1:others], s_sem.at[0, w])
+        slab_wait(csend.at[w, 1:others], e_sem.at[0, w])
 
     final = None
     for w in range(waves):
-        for t in range(n_tp):
-            if t:
-                slab_wait(crecv.at[w, t], e_rs.at[w, t])
-            else:
-                for e in range(1, n_ep):
-                    slab_wait(crecv.at[w, 0, e], e0_rs.at[w, e])
+        slab_wait(crecv.at[w, 1:others], e_sem.at[1, w])
         routed = [jnp.zeros((ROWS, colsp), F32) for _ in range(pack)]
         for g in range(n_groups):
             total = jnp.zeros((ROWS, colsp), F32)
             for m in range(EPG):
-                e = g * EPG + m
-                out = crecv[w, 0, e].astype(F32)
+                e = lax.rem(g * EPG + m - ep + n_ep, n_ep)
+                out = crecv[w, e].astype(F32)
                 for t in range(1, n_tp):
-                    out = out + crecv[w, t, e].astype(F32)
+                    out = out + crecv[w, t * n_ep + e].astype(F32)
                 total = total + weights_of[w][g][m] * out.astype(BF16).astype(F32)
             for p in range(pack):
                 routed[p] = jnp.where(rows_of // hc == g, roll_rows(total, g * hc - p * hc), routed[p])
@@ -444,6 +419,7 @@
     hc = ROWS // n_groups
     pack = 2 if hc * 2 == ROWS and cols % 256 == 0 else 1
     colsp = cols // pack
+    devices = n_ep * n_tp
     vmem = pl.BlockSpec(memory_space=pltpu.VMEM)
     hbm = pl.BlockSpec(memory_space=pl.ANY)
     dma = pltpu.SemaphoreType.DMA
@@ -470,17 +446,13 @@
         pltpu.VMEM((waves, n_tp, ROWS, cols), BF16),
         pltpu.VMEM((waves, n_tp, ROWS, cols), BF16),
         pltpu.VMEM((waves, n_groups, ROWS, colsp), BF16),
-        pltpu.VMEM((waves, n_tp, n_ep, ROWS, colsp), BF16),
+        pltpu.VMEM((waves, devices, ROWS, colsp), BF16),
         pltpu.VMEM((waves, 1, 128), F32),
-        pltpu.VMEM((waves, n_tp, n_ep, 1, 128), F32),
-        pltpu.VMEM((waves, n_tp, n_ep, ROWS, colsp), BF16),
-        pltpu.VMEM((waves, n_tp, n_ep, ROWS, colsp), BF16),
-        dma((11,)), dma((7,)), dma((2, seqs // LOAD)),
-        dma((n_ep,)), dma((n_ep,)), dma((2, n_ep)), dma((2, n_ep)),
-        dma((waves, n_tp)), dma((waves, n_tp)),
-        dma((waves, n_tp, n_ep)), dma((waves, n_tp)), dma((waves, n_ep)),
-        dma((waves, n_tp, n_ep)), dma((waves, n_tp)), dma((waves, n_ep)),
-        dma((waves, n_tp, n_ep)), dma((waves, n_tp)), dma((waves, n_ep)),
+        pltpu.VMEM((waves, devices, 1, 128), F32),
+        pltpu.VMEM((waves, devices, ROWS, colsp), BF16),
+        pltpu.VMEM((waves, devices, ROWS, colsp), BF16),
+        dma((11,)), dma((7,)), dma((seqs // LOAD + 1,)), dma((2,)), dma((4,)), dma((2, waves)),
+        dma((waves,)), dma((waves, 4)), dma((2, waves)), dma((2, waves)),
     ]
     shapes = (
         jax.ShapeDtypeStruct((seqs, cols), BF16),

time: 40.9 us -> 38.2 us (0.934)
  Pallas kernels: 40 us -> 37.4 us
    pallas_call x1, Pallas kernels: 38.7 us -> 36 us  [on_device(): pl.pallas_call(functools.partial(layer_kernel, n_ep, n_tp), out_shape=sha...]
where the time goes in v2:
time: 38.2 us; the launch traced here: 38 us
  Pallas kernels  37.4 us (98%)
  between operations  0.65 us (2%)
    pallas_call x1, Pallas kernels, on_device(): pl.pallas_call(functools.partial(layer_kernel, n_ep, n_tp), out_shape=sha...  36 us
    pallas_call x1, Pallas kernels, on_device(): pl.pallas_call(finish_kernel, out_shape=shapes, in_specs=[vmem] * 3, out_...  1.35 us

profile of v2, /device:TPU:0, one launch (start us, length us, event | category | flops | bytes accessed | tf_op | source)
XLA Modules:
  0.0 38.0 jit_solution(15137693584822523391)
XLA Ops:
  0.6 36.0 %decode_layer.1 = (bf16[16,512]{1,0:T(8,128)(2,1)}, bf16[16,256]{1,0:T(8,128)(2,1)}, bf16[16,256]{1,0:T(8,128)(2,1)}) custom-call(bf16[16,4096]{1,0:T(8,128)(2,1)} %tokens_h.1, f32[1,4096]{1,0:T(1,128)} %bitcast.7, f32[1,128]{1,0:T(1,128)} %bitcast.12, f32[1,4096]{1,0:T(1,128)} %bitcast.8, f32[2]{0:T(128)} %lam_h.1, s32[16]{0:T(128)} %lengths_h.1, ...), custom_call_target="tpu_custom_call" | custom-call | tf_op jit(solution)/shard_map/decode_layer/pallas_call | solution.py:462
  36.7 1.4 %finish.1 = (bf16[16,512]{1,0:T(8,128)(2,1)}, bf16[16,256]{1,0:T(8,128)(2,1)}, bf16[16,256]{1,0:T(8,128)(2,1)}) custom-call(bf16[16,512]{1,0:T(8,128)(2,1)} %get-tuple-element.6.a, bf16[16,256]{1,0:T(8,128)(2,1)} %get-tuple-element.7.b, bf16[16,256]{1,0:T(8,128)(2,1)} %get-tuple-element.8.c), custom_call_target="tpu_custom_call" | custom-call | tf_op jit(solution)/shard_map/finish/pallas_call | solution.py:473

commit v3 on v2

--- a/solution.py
+++ b/solution.py
@@ -14,6 +14,7 @@
 BF16 = jnp.bfloat16
 LOAD = 4
 ROWS = 8
+LANES = 128
 
 
 def iota(shape, dim):
@@ -37,8 +38,8 @@
     tokens, attn_gain, head_gain, moe_gain, lam, lengths, groups, groups_row, members, group_gate, logits,
     wq, wk, wv, kbuf, vbuf, ktrans, wo, wg, wu, wd,
     nsend, nrecv, qpart, kvpart, qprecv, kvprecv, mixbuf,
-    tsend, trecv, dsend, drecv, ssend, srecv, csend, crecv,
-    i_sem, w_sem, c_sem, n_sem, p_sem, t_sem, d_ss, d_rs, s_sem, e_sem,
+    tsend, trecv, dsend, drecv, ssend, srecv, spart, sother, csend, crecv,
+    i_sem, w_sem, c_sem, n_sem, p_sem, t_sem, d_ss, d_rs, f_sem, s_sem, g_sem, e_sem, known,
 ):
     ep = lax.axis_index("ep")
     tp = lax.axis_index("tp")
@@ -63,7 +64,8 @@
     ot = [lax.rem(tp + d, n_tp) for d in range(n_tp)]
 
     barrier = pltpu.get_barrier_semaphore()
-    for d in range(1, n_tp):
+    near = sorted({1, n_tp - 1})
+    for d in near:
         pl.semaphore_signal(barrier, inc=1, device_id={"ep": ep, "tp": ot[d]}, device_id_type=MESH)
     for d in range(1, n_ep):
         pl.semaphore_signal(barrier, inc=1, device_id={"ep": oe[d], "tp": tp}, device_id_type=MESH)
@@ -76,7 +78,10 @@
     small_copies = [pltpu.make_async_copy(s, d, i_sem.at[i]) for i, (s, d) in enumerate(small)]
     for c in small_copies:
         c.start()
-    weight_pairs = [(w_query, wq), (w_key, wk), (w_value, wv), (w_output, wo), (w_gate, wg), (w_up, wu), (w_down, wd)]
+    weight_pairs = [
+        (w_query, wq), (w_key, wk), (w_value, wv), (w_output, wo.at[:, :width]), (w_gate, wg), (w_up, wu),
+        (w_down, wd.at[:, :, :width]),
+    ]
     weight_copies = [pltpu.make_async_copy(s, d, w_sem.at[i]) for i, (s, d) in enumerate(weight_pairs)]
 
     def key_copy(g):
@@ -106,19 +111,32 @@
             src_ref=src, dst_ref=dst, send_sem=ss, recv_sem=rs, device_id={"ep": e, "tp": t}, device_id_type=MESH
         )
 
-    pl.semaphore_wait(barrier, n_ep + n_tp - 2)
+    pl.semaphore_wait(barrier, n_ep - 1 + len(near))
+    hops = [1 << k for k in range((n_tp // 2).bit_length() - 1)]
+
+    def tell(k):
+        for side in range(2):
+            at = ot[hops[k] if side else n_tp - hops[k]]
+            pl.semaphore_signal(known.at[k, side], inc=1, device_id={"ep": ep, "tp": at}, device_id_type=MESH)
+
+    def hear(k):
+        for side in range(2):
+            pl.semaphore_wait(known.at[k, side], 1)
+
     def slab_wait(ref, sem):
         pltpu.make_async_copy(ref, ref, sem).wait()
 
     for d in range(1, n_ep):
         remote(nsend.at[oe[d]], nrecv.at[d], n_sem.at[0], n_sem.at[1], oe[d], tp).start()
+    if hops:
+        tell(0)
     nrecv[0] = nsend[ep]
 
     eye = (iota((qk_cols, qk_cols), 0) == iota((qk_cols, qk_cols), 1)).astype(BF16)
 
     def turn(s, carry):
         flipped = lax.dot_general(eye, kbuf[s], (((1,), (1,)), ((), ())), preferred_element_type=F32)
-        ktrans[s] = flipped.astype(BF16)
+        ktrans[s, :, :positions] = flipped.astype(BF16)
         return carry
 
     def turn_group(g, carry):
@@ -132,6 +150,9 @@
     for c in weight_copies[:3]:
         c.wait()
     slab_wait(nrecv.at[1:n_ep], n_sem.at[1])
+    for k in range(len(hops) - 1):
+        hear(k)
+        tell(k + 1)
     rows_all = nrecv[...].reshape(n_ep * seqs, rows_local)
     for i, w in enumerate((wq, wk, wv)):
         part = mm(rows_all, w[...]).reshape(n_ep, seqs, qk_cols)
@@ -219,6 +240,8 @@
     pick16 = (row_id % ROWS) // heads_local
 
     value_copy.wait()
+    if hops:
+        hear(len(hops) - 1)
 
     slab_wait(qprecv.at[1:n_ep], p_sem.at[1])
     slab_wait(kvprecv.at[1:n_ep], p_sem.at[3])
@@ -234,7 +257,7 @@
 
     weight_copies[3].wait()
 
-    def attend(base):
+    def score(base):
         wanted = (base + pick16).astype(F32)
         spread = mm((place_row == wanted).astype(BF16), projected)
         q16 = spread[:, :qk_cols] * map_mask
@@ -244,9 +267,12 @@
             at = perm[base + i]
             lens = jnp.where(pick16 == i, lengths[at], lens)
             own = jnp.where(seq16 == i, q16, 0.0).astype(BF16)
-            part = mm(own, ktrans[at])
+            part = mm(own, ktrans[at, :, :positions])
             old = part if old is None else old + part
         new = jnp.sum(q16 * spread[:, qk_cols : 2 * qk_cols], axis=-1, keepdims=True) * scale
+        return old, new, lens, spread[:ROWS, 2 * qk_cols :]
+
+    def weigh(old, new, lens, value):
         old = old * scale - slopes * (lens - spots).astype(F32)
         old = jnp.where(spots < lens, old, -jnp.inf)
         top = jnp.maximum(jnp.max(old, axis=-1, keepdims=True), new)
@@ -257,7 +283,9 @@
         new = new * recip
         weights = (old[:ROWS] - lam_col * old[ROWS:]).astype(BF16)
         fresh_weight = (new[:ROWS] - lam_col * new[ROWS:]).astype(BF16).astype(F32)
-        mix = fresh_weight * spread[:ROWS, 2 * qk_cols :]
+        return weights, fresh_weight * value
+
+    def combine(base, weights, mix):
         for i in range(batch):
             part = mm(weights, vbuf[perm[base + i]])
             mix = mix + jnp.where(seq8 == i, part, 0.0)
@@ -265,10 +293,8 @@
         mean = jnp.sum(mix * mix, axis=-1, keepdims=True) / pair
         return mix * lax.rsqrt(mean + EPS) * gain_row
 
-    for w in range(waves):
-        per_wave = ROWS // batch
-        for k in range(per_wave):
-            mix = attend(w * ROWS + k * batch)
+    def project(w, mixes):
+        for k, mix in enumerate(mixes):
             for h in range(heads_local):
                 mixbuf[w * heads_local + h, k * ROWS : (k + 1) * ROWS, :] = mix[:, h * pair : (h + 1) * pair]
         heads = [
@@ -280,14 +306,44 @@
             term = mm(heads, block).astype(BF16)
             if d:
                 tsend[w, d] = term
-                remote(tsend.at[w, d], trecv.at[w, d], t_sem.at[0, w], t_sem.at[1, w], ep, ot[d]).start()
             else:
                 trecv[w, 0] = term
+        for d in range(1, n_tp):
+            remote(tsend.at[w, d], trecv.at[w, d], t_sem.at[0, w], t_sem.at[1, w], ep, ot[d]).start()
+
+    per_wave = ROWS // batch
+    steps = seqs // batch
+    scores = {}
+    ready = {}
+    mixes = []
+
+    def prepare(k):
+        if k < steps and k not in scores:
+            scores[k] = score(k * batch)
+
+    prepare(0)
+    for k in range(steps):
+        prepare(k + 1)
+        ready[k] = weigh(*scores[k])
+        if k % per_wave == per_wave - 1:
+            prepare(k + 1)
+        mixes.append(combine(k * batch, *ready[k]))
+        if k % per_wave == per_wave - 1:
+            project(k // per_wave, mixes[-per_wave:])
 
     rows_of = iota((ROWS, colsp), 0)
     resid = []
-    parts = d_rs.shape[1]
     others = n_tp * n_ep
+    cores = 2
+    floors = n_tp // cores
+    core = lax.rem(tp, cores)
+    floor = tp // cores
+    sibling = tp + 1 - 2 * core
+    half_slots = floors * n_ep
+    up = [lax.rem(floor + d, floors) * cores + core for d in range(floors)]
+    down_floor = [lax.rem(floor + floors - d, floors) * cores for d in range(floors)]
+    far_first = sorted(range(1, floors), key=lambda d: (-min(d, floors - d), d)) + [0]
+    near_first = far_first[::-1]
     for w in range(waves):
         slab_wait(trecv.at[w, 1:n_tp], t_sem.at[1, w])
         attn = trecv[w, 0].astype(F32)
@@ -306,13 +362,12 @@
         squares = jnp.sum(res * res, axis=-1, keepdims=True)
         wide = jnp.where(iota((ROWS, 128), 0) == iota((ROWS, 128), 1), squares, 0.0)
         ssend[w] = jnp.sum(wide, axis=0, keepdims=True)
-        for t in [*range(1, n_tp), 0]:
+        for d in far_first:
             for e in range(n_ep):
-                if t or e:
-                    at = t * n_ep + e
-                    arrived = d_rs.at[w, t * parts // n_tp]
-                    remote(dsend.at[w, oe[e] // EPG], drecv.at[w, at], d_ss.at[w], arrived, oe[e], ot[t]).start()
-                    remote(ssend.at[w], srecv.at[w, at], s_sem.at[0, w], s_sem.at[1, w], oe[e], ot[t]).start()
+                if d or e:
+                    at = d * n_ep + e
+                    remote(dsend.at[w, oe[e] // EPG], drecv.at[w, at], d_ss.at[w], d_rs.at[w, d], oe[e], up[d]).start()
+                    remote(ssend.at[w], srecv.at[w, at], s_sem.at[0, w], s_sem.at[1, w], oe[e], up[d]).start()
         drecv[w, 0] = dsend[w, ep // EPG]
         srecv[w, 0] = ssend[w]
 
@@ -323,20 +378,32 @@
         hid = w_gate.shape[2]
         gates = [jnp.zeros((slots, hid), F32) for _ in range(pack)]
         uppers = [jnp.zeros((slots, hid), F32) for _ in range(pack)]
-        for t in range(n_tp):
-            step = n_tp // parts
-            if t % step == 0:
-                slab_wait(drecv.at[w, max(t * n_ep, 1) : (t + step) * n_ep], d_rs.at[w, t // step])
-            x = drecv[w, t * n_ep : (t + 1) * n_ep].reshape(slots, colsp)
-            source = lax.rem(tp + n_tp - t, n_tp)
+        def feed(slot, source):
+            x = drecv[w, slot * n_ep : (slot + 1) * n_ep].reshape(slots, colsp)
             for p in range(pack):
                 at = pl.ds(pl.multiple_of(source * cols + p * colsp, colsp), colsp)
                 gates[p] = gates[p] + mm(x, wg[0, at])
                 uppers[p] = uppers[p] + mm(x, wu[0, at])
-        slab_wait(srecv.at[w, 1:others], s_sem.at[1, w])
+
+        for d in near_first:
+            slab_wait(drecv.at[w, max(d * n_ep, 1) : (d + 1) * n_ep], d_rs.at[w, d])
+            remote(
+                drecv.at[w, d * n_ep : (d + 1) * n_ep], drecv.at[w, half_slots + d * n_ep : half_slots + (d + 1) * n_ep],
+                f_sem.at[0, w], f_sem.at[1, w], ep, sibling,
+            ).start()
+        slab_wait(srecv.at[w, 1:half_slots], s_sem.at[1, w])
         squares = srecv[w, 0:n_ep]
-        for t in range(1, n_tp):
-            squares = squares + srecv[w, t * n_ep : (t + 1) * n_ep]
+        for d in range(1, floors):
+            squares = squares + srecv[w, d * n_ep : (d + 1) * n_ep]
+        spart[w] = squares
+        remote(spart.at[w], sother.at[w], g_sem.at[0, w], g_sem.at[1, w], ep, sibling).start()
+        for d in near_first:
+            feed(d, down_floor[d] + core)
+        slab_wait(drecv.at[w, half_slots:], f_sem.at[1, w])
+        for d in near_first:
+            feed(floors + d, down_floor[d] + 1 - core)
+        slab_wait(sother.at[w], g_sem.at[1, w])
+        squares = squares + sother[w]
         squares = jnp.broadcast_to(squares, (n_ep, ROWS, 128)).reshape(slots, 128)
         slot = iota((slots, 128), 0) % ROWS
         if pack == 2:
@@ -363,6 +430,7 @@
             down = downs[0] if pack == 1 else jnp.where(iota((slots, colsp), 0) % ROWS < hc, downs[0], downs[1])
             down = down.reshape(n_ep, ROWS, colsp).astype(BF16)
             csend[w, t * n_ep : (t + 1) * n_ep] = down
+        for t in [*range(1, n_tp), 0]:
             for e in range(n_ep):
                 if t or e:
                     at = t * n_ep + e
@@ -374,8 +442,10 @@
     slab_wait(kvpart.at[1:n_ep], p_sem.at[2])
     for w in range(waves):
         slab_wait(tsend.at[w, 1:n_tp], t_sem.at[0, w])
-        slab_wait(drecv.at[w, 1:others], d_ss.at[w])
-        slab_wait(srecv.at[w, 1:others], s_sem.at[0, w])
+        slab_wait(drecv.at[w, 1:half_slots], d_ss.at[w])
+        slab_wait(drecv.at[w, half_slots:], f_sem.at[0, w])
+        slab_wait(srecv.at[w, 1:half_slots], s_sem.at[0, w])
+        slab_wait(spart.at[w], g_sem.at[0, w])
         slab_wait(csend.at[w, 1:others], e_sem.at[0, w])
 
     final = None
@@ -424,6 +494,7 @@
     hbm = pl.BlockSpec(memory_space=pl.ANY)
     dma = pltpu.SemaphoreType.DMA
     like = lambda a: pltpu.VMEM(a.shape, a.dtype)
+    padded = lambda a: pltpu.VMEM((*a.shape[:-1], a.shape[-1] + LANES), a.dtype)
     operands = (
         tokens, attn_gain[None, :], head_gain[None, :], moe_gain[None, :], mix_lambda, lengths, group_ids,
         group_ids[None, :], member_ids.T, group_gate[None, :], member_logits.T,
@@ -434,8 +505,8 @@
     ]
     scratch = held + [
         like(w_query), like(w_key), like(w_value), like(cache_keys), like(cache_value),
-        pltpu.VMEM((seqs, qk_cols, cache_keys.shape[1]), BF16),
-        like(w_output), like(w_exp_gate), like(w_exp_up), like(w_exp_down),
+        pltpu.VMEM((seqs, qk_cols, cache_keys.shape[1] + LANES), BF16),
+        padded(w_output), like(w_exp_gate), like(w_exp_up), padded(w_exp_down),
         pltpu.VMEM((n_ep, seqs, width // n_ep), BF16),
         pltpu.VMEM((n_ep, seqs, width // n_ep), BF16),
         pltpu.VMEM((n_ep, seqs, qk_cols), F32),
@@ -448,11 +519,14 @@
         pltpu.VMEM((waves, n_groups, ROWS, colsp), BF16),
         pltpu.VMEM((waves, devices, ROWS, colsp), BF16),
         pltpu.VMEM((waves, 1, 128), F32),
-        pltpu.VMEM((waves, devices, 1, 128), F32),
+        pltpu.VMEM((waves, devices // 2, 1, 128), F32),
+        pltpu.VMEM((waves, n_ep, 1, 128), F32),
+        pltpu.VMEM((waves, n_ep, 1, 128), F32),
         pltpu.VMEM((waves, devices, ROWS, colsp), BF16),
         pltpu.VMEM((waves, devices, ROWS, colsp), BF16),
         dma((11,)), dma((7,)), dma((seqs // LOAD + 1,)), dma((2,)), dma((4,)), dma((2, waves)),
-        dma((waves,)), dma((waves, 4)), dma((2, waves)), dma((2, waves)),
+        dma((waves,)), dma((waves, n_tp // 2)), dma((2, waves)), dma((2, waves)), dma((2, waves)), dma((2, waves)),
+        pltpu.SemaphoreType.REGULAR((max((n_tp // 2).bit_length() - 1, 1), 2)),
     ]
     shapes = (
         jax.ShapeDtypeStruct((seqs, cols), BF16),

time: 38.2 us -> 36.9 us (0.966)
  Pallas kernels: 37.4 us -> 36 us
    pallas_call x1, Pallas kernels: 36 us -> 34.7 us  [on_device(): pl.pallas_call(functools.partial(layer_kernel, n_ep, n_tp), out_shape=sha...]
where the time goes in v3:
time: 36.9 us; the launch traced here: 36.7 us
  Pallas kernels  36 us (98%)
  between operations  0.65 us (2%)
    pallas_call x1, Pallas kernels, on_device(): pl.pallas_call(functools.partial(layer_kernel, n_ep, n_tp), out_shape=sha...  34.7 us
    pallas_call x1, Pallas kernels, on_device(): pl.pallas_call(finish_kernel, out_shape=shapes, in_specs=[vmem] * 3, out_...  1.35 us

profile of v3, /device:TPU:0, one launch (start us, length us, event | category | flops | bytes accessed | tf_op | source)
XLA Modules:
  0.0 36.7 jit_solution(12822018837897174883)
XLA Ops:
  0.6 34.7 %decode_layer.1 = (bf16[16,512]{1,0:T(8,128)(2,1)}, bf16[16,256]{1,0:T(8,128)(2,1)}, bf16[16,256]{1,0:T(8,128)(2,1)}) custom-call(bf16[16,4096]{1,0:T(8,128)(2,1)} %tokens_h.1, f32[1,4096]{1,0:T(1,128)} %bitcast.7, f32[1,128]{1,0:T(1,128)} %bitcast.12, f32[1,4096]{1,0:T(1,128)} %bitcast.8, f32[2]{0:T(128)} %lam_h.1, s32[16]{0:T(128)} %lengths_h.1, ...), custom_call_target="tpu_custom_call" | custom-call | tf_op jit(solution)/shard_map/decode_layer/pallas_call | solution.py:536
  35.3 1.4 %finish.1 = (bf16[16,512]{1,0:T(8,128)(2,1)}, bf16[16,256]{1,0:T(8,128)(2,1)}, bf16[16,256]{1,0:T(8,128)(2,1)}) custom-call(bf16[16,512]{1,0:T(8,128)(2,1)} %get-tuple-element.6.a, bf16[16,256]{1,0:T(8,128)(2,1)} %get-tuple-element.7.b, bf16[16,256]{1,0:T(8,128)(2,1)} %get-tuple-element.8.c), custom_call_target="tpu_custom_call" | custom-call | tf_op jit(solution)/shard_map/finish/pallas_call | solution.py:547

commit v4 on v3

--- a/solution.py
+++ b/solution.py
@@ -64,11 +64,11 @@
     ot = [lax.rem(tp + d, n_tp) for d in range(n_tp)]
 
     barrier = pltpu.get_barrier_semaphore()
+    for d in range(1, n_ep):
+        pl.semaphore_signal(barrier, inc=1, device_id={"ep": oe[d], "tp": tp}, device_id_type=MESH)
     near = sorted({1, n_tp - 1})
     for d in near:
         pl.semaphore_signal(barrier, inc=1, device_id={"ep": ep, "tp": ot[d]}, device_id_type=MESH)
-    for d in range(1, n_ep):
-        pl.semaphore_signal(barrier, inc=1, device_id={"ep": oe[d], "tp": tp}, device_id_type=MESH)
 
     small = [
         (tokens_h, tokens), (attn_gain_h, attn_gain), (head_gain_h, head_gain), (moe_gain_h, moe_gain), (lam_h, lam),
@@ -150,9 +150,6 @@
     for c in weight_copies[:3]:
         c.wait()
     slab_wait(nrecv.at[1:n_ep], n_sem.at[1])
-    for k in range(len(hops) - 1):
-        hear(k)
-        tell(k + 1)
     rows_all = nrecv[...].reshape(n_ep * seqs, rows_local)
     for i, w in enumerate((wq, wk, wv)):
         part = mm(rows_all, w[...]).reshape(n_ep, seqs, qk_cols)
@@ -165,6 +162,9 @@
         remote(qpart.at[d], qprecv.at[d], p_sem.at[0], p_sem.at[1], back[d], tp).start()
         remote(kvpart.at[d], kvprecv.at[d], p_sem.at[2], p_sem.at[3], back[d], tp).start()
 
+    for k in range(len(hops) - 1):
+        hear(k)
+        tell(k + 1)
     lax.fori_loop(half, seqs // LOAD, turn_group, 0)
 
     for c in small_copies[2:]:
@@ -257,9 +257,12 @@
 
     weight_copies[3].wait()
 
+    row_all = iota((seqs // batch * 2 * ROWS, 1), 0)
+    wanted = (row_all // (2 * ROWS)) * batch + (row_all % ROWS) // heads_local
+    spread_all = mm((place_row == wanted.astype(F32)).astype(BF16), projected)
+
     def score(base):
-        wanted = (base + pick16).astype(F32)
-        spread = mm((place_row == wanted).astype(BF16), projected)
+        spread = spread_all[base // batch * 2 * ROWS : (base // batch + 1) * 2 * ROWS]
         q16 = spread[:, :qk_cols] * map_mask
         lens = jnp.zeros((2 * ROWS, 1), jnp.int32)
         old = None

time: 36.9 us -> 36.7 us (level)
  no operation moved by 1% of the time
where the time goes in v4:
time: 36.7 us; the launch traced here: 36.5 us
  Pallas kernels  35.8 us (98%)
  between operations  0.65 us (2%)
    pallas_call x1, Pallas kernels, on_device(): pl.pallas_call(functools.partial(layer_kernel, n_ep, n_tp), out_shape=sha...  34.5 us
    pallas_call x1, Pallas kernels, on_device(): pl.pallas_call(finish_kernel, out_shape=shapes, in_specs=[vmem] * 3, out_...  1.35 us

profile of v4, /device:TPU:0, one launch (start us, length us, event | category | flops | bytes accessed | tf_op | source)
XLA Modules:
  0.0 36.5 jit_solution(11845638702706363256)
XLA Ops:
  0.6 34.5 %decode_layer.1 = (bf16[16,512]{1,0:T(8,128)(2,1)}, bf16[16,256]{1,0:T(8,128)(2,1)}, bf16[16,256]{1,0:T(8,128)(2,1)}) custom-call(bf16[16,4096]{1,0:T(8,128)(2,1)} %tokens_h.1, f32[1,4096]{1,0:T(1,128)} %bitcast.7, f32[1,128]{1,0:T(1,128)} %bitcast.12, f32[1,4096]{1,0:T(1,128)} %bitcast.8, f32[2]{0:T(128)} %lam_h.1, s32[16]{0:T(128)} %lengths_h.1, ...), custom_call_target="tpu_custom_call" | custom-call | tf_op jit(solution)/shard_map/decode_layer/pallas_call | solution.py:539
  35.1 1.4 %finish.1 = (bf16[16,512]{1,0:T(8,128)(2,1)}, bf16[16,256]{1,0:T(8,128)(2,1)}, bf16[16,256]{1,0:T(8,128)(2,1)}) custom-call(bf16[16,512]{1,0:T(8,128)(2,1)} %get-tuple-element.6.a, bf16[16,256]{1,0:T(8,128)(2,1)} %get-tuple-element.7.b, bf16[16,256]{1,0:T(8,128)(2,1)} %get-tuple-element.8.c), custom_call_target="tpu_custom_call" | custom-call | tf_op jit(solution)/shard_map/finish/pallas_call | solution.py:550
